TPU v7x, 512 devices: a whole 4x4x16 slice. The times are simulated.
512 devices in a mesh: sp: 64 (over z, y), tp: 8 (over x, core).
Axes of the slice: x: 4, y: 4, z: 16, core: 2. Of those that a mesh axis runs over, the one named last changes fastest.
Arguments:
- tokens: bfloat16 [65536, 2048], P('sp', 'tp'), may hold values from -6 to 6
- norm_gain: float32 [2048], replicated, may hold values from 0.1 to 1.9
- w_query: bfloat16 [2048, 1024], P('sp', 'tp'), may hold values from -0.125 to 0.125
- w_key: bfloat16 [2048, 512], P('sp', 'tp'), may hold values from -0.125 to 0.125
- w_value: bfloat16 [2048, 512], P('sp', 'tp'), may hold values from -0.125 to 0.125
- w_glu_a: bfloat16 [2048, 1024], P('sp', 'tp'), may hold values from -0.125 to 0.125
- w_glu_b: bfloat16 [2048, 1024], P('sp', 'tp'), may hold values from -0.125 to 0.125
- q_gain: float32 [64], replicated, may hold values from 0.8 to 7
- k_gain: float32 [64], replicated, may hold values from 0.8 to 7
- sink_logit: float32 [16], P('tp'), may hold values from 1 to 4
- conv_taps: float32 [31, 1024], P(None, 'tp'), may hold values from -1 to 1
- chan_gain: float32 [1024], P('tp'), may hold values from 0.1 to 1.9
- chan_bias: float32 [1024], P('tp'), may hold values from -3 to 3
- w_attn_back: bfloat16 [2048, 1024], P('sp', 'tp'), may hold values from -0.1875 to 0.1875
- w_conv_back: bfloat16 [2048, 1024], P('sp', 'tp'), may hold values from -0.1875 to 0.1875
Outputs:
- mixed: bfloat16 [65536, 2048], P(('sp', 'tp'))
- log_weight: float32 [16, 65536], P('tp', 'sp')
All inputs are finite; a program needn't handle non-finite values.
Results may differ from a plain program's by a relative error of at most 0.014.
The roundings to bfloat16 on the way count: a program that leaves them out, or rounds other values in their place, can miss the bound.
Values may be sent and summed in bfloat16 or wider, within the bound.
A program may use at most 128 MiB of HBM per device.

v0:
```python
import jax
import jax.numpy as jnp
from jax import lax
from jax.sharding import Mesh
from jax.sharding import PartitionSpec as P

HEAD = 64
CH = 1024
KW = 31
WINDOW = 128
TP = ("tp_0", "tp_1")
SP_TP = ("sp", "tp_0", "tp_1")


EPS = 1e-06


def sent_to_all(array, axis):
    copies = jnp.broadcast_to(array, (lax.axis_size(axis), *array.shape))
    return lax.all_to_all(copies, axis, split_axis=0, concat_axis=0, tiled=True)


def laid_out(tiles, dim):
    lengths = list(tiles.shape[1:])
    lengths[dim] *= tiles.shape[0]
    return jnp.moveaxis(tiles, 0, dim).reshape(lengths)


def gathered_by_axis(array, axes, dim):
    far, near = axes
    leading = sent_to_all(array, far)
    tiles = jnp.swapaxes(sent_to_all(leading, near), 0, 1)
    return laid_out(tiles.reshape(-1, *array.shape), dim)


def side_by_side(arrays, axis, dim, along):
    both = jnp.concatenate(arrays, axis=along)
    whole, at, outs = (lax.all_gather(both, axis, axis=dim, tiled=True), 0, [])
    for a in arrays:
        outs.append(lax.slice_in_dim(whole, at, at + a.shape[along], axis=along))
        at += a.shape[along]
    return tuple(outs)


def passed_along(value, axis, steps):
    count = lax.axis_size(axis)
    leading, last = (max(0, -steps), min(count, count - steps))
    return lax.ppermute(value, axis, [(source, source + steps) for source in range(leading, last)])


def taken_together(array, axis):
    return sent_to_all(array, axis).sum(axis=0)


def together(arrays, axis):
    ends = [0]
    for a in arrays:
        ends.append(ends[-1] + a.size)
    running = taken_together(jnp.concatenate([a.ravel() for a in arrays]), axis)
    return tuple((running[b:e].reshape(a.shape) for a, b, e in zip(arrays, ends, ends[1:])))


def row_norm(inputs, scale_vec):
    squares = jnp.mean(inputs * inputs, axis=-1, keepdims=True)
    return inputs * lax.rsqrt(squares + EPS) * scale_vec


def local(
    tokens,
    norm_gain,
    w_query,
    w_key,
    w_value,
    w_glu_a,
    w_glu_b,
    q_gain,
    k_gain,
    sink_logit,
    conv_taps,
    chan_gain,
    chan_bias,
    w_attn_back,
    w_conv_back,
):
    row_count = tokens.shape[0]
    q_local = w_query.shape[1] // HEAD
    kv_local = w_key.shape[1] // HEAD
    group_size = q_local // kv_local
    kv_width = kv_local * HEAD
    gathered = gathered_by_axis(tokens, ("tp_0", "tp_1"), 1)
    normed = row_norm(gathered.astype(jnp.float32), norm_gain).astype(jnp.bfloat16)
    whole_rows = side_by_side(
        (w_query, w_key, w_value, w_glu_a, w_glu_b, w_attn_back, w_conv_back), "sp", 0, 1
    )
    projected = tuple(
        (jnp.dot(normed, weight, preferred_element_type=jnp.float32) for weight in whole_rows[:5])
    )
    attn_back = whole_rows[5]
    conv_back = whole_rows[6]
    query_raw, key_raw, value_raw, glu_a, glu_b = projected
    queries = row_norm(query_raw.reshape(row_count, q_local, HEAD), q_gain).astype(jnp.bfloat16)
    key_rows = (
        row_norm(key_raw.reshape(row_count, kv_local, HEAD), k_gain)
        .astype(jnp.bfloat16)
        .reshape(row_count, kv_width)
    )
    value_rows = value_raw.astype(jnp.bfloat16)
    gated_rows = (glu_a * jax.nn.sigmoid(glu_b)).astype(jnp.bfloat16)
    key_value = jnp.concatenate([key_rows, value_rows], 1)
    key_value_rim = passed_along(key_value[row_count - WINDOW :], "sp", 1)
    gated_rim = passed_along(gated_rows[row_count - (KW - 1) :], "sp", 1)
    block_count = row_count // WINDOW
    extended = jnp.concatenate([key_value_rim, key_value], 0).reshape(
        block_count + 1, WINDOW, 2 * kv_width
    )
    band = jnp.concatenate([extended[:-1], extended[1:]], 1)
    key_band = band[:, :, :kv_width].reshape(block_count, 2 * WINDOW, kv_local, HEAD)
    value_band = band[:, :, kv_width:].reshape(block_count, 2 * WINDOW, kv_local, HEAD)
    grouped = queries.reshape(block_count, WINDOW, kv_local, group_size, HEAD)
    scores = jnp.einsum(
        "nqhgd,nkhd->nhgqk", grouped, key_band, preferred_element_type=jnp.float32
    ) * HEAD ** (-0.5)
    offsets = jnp.arange(WINDOW, dtype=jnp.int32)
    band_offsets = jnp.arange(2 * WINDOW, dtype=jnp.int32)
    distance = WINDOW + offsets[:, None] - band_offsets[None, :]
    allowed = (distance >= 0) & (distance < WINDOW)
    anchor = lax.axis_index("sp") * row_count
    key_position = (
        anchor
        + jnp.arange(block_count, dtype=jnp.int32)[:, None] * WINDOW
        - WINDOW
        + band_offsets[None, :]
    )
    visible = (allowed[None, :, :] & (key_position[:, None, :] >= 0))[:, None, None]
    sink_table = sink_logit.reshape(kv_local, group_size)[None, :, :, None, None]
    masked = jnp.where(visible, scores, -jnp.inf)
    largest = jnp.maximum(jnp.max(masked, axis=-1, keepdims=True), sink_table)
    weights = jnp.where(visible, jnp.exp(scores - largest), 0.0)
    weight_sum = jnp.sum(weights, axis=-1, keepdims=True) + jnp.exp(sink_table - largest)
    log_weight = (largest + jnp.log(weight_sum))[..., 0]
    log_weight = jnp.transpose(log_weight, (1, 2, 0, 3)).reshape(q_local, row_count)
    probabilities = (weights / weight_sum).astype(jnp.bfloat16)
    attended = jnp.einsum(
        "nhgqk,nkhd->nqhgd", probabilities, value_band, preferred_element_type=jnp.float32
    )
    attended = attended.astype(jnp.bfloat16).reshape(row_count, q_local * HEAD)
    gate_extended = jnp.concatenate([gated_rim, gated_rows], 0).astype(jnp.float32)
    convolved = jnp.zeros((row_count, gated_rows.shape[1]), jnp.float32)
    for tap_index in range(KW):
        convolved = (
            convolved + conv_taps[tap_index] * gate_extended[tap_index : tap_index + row_count]
        )
    channel_sums = together(
        (jnp.sum(convolved, axis=1), jnp.sum(convolved * convolved, axis=1)), TP
    )
    center = (channel_sums[0] / CH)[:, None]
    spread = (channel_sums[1] / CH)[:, None] - center * center
    conv_rows = jax.nn.silu(
        (convolved - center) * lax.rsqrt(spread + EPS) * chan_gain + chan_bias
    ).astype(jnp.bfloat16)
    contract = (((1,), (1,)), ((), ()))
    result = lax.dot_general(attended, attn_back, contract, preferred_element_type=jnp.float32)
    summed = lax.psum_scatter(
        (
            result
            + lax.dot_general(conv_rows, conv_back, contract, preferred_element_type=jnp.float32)
        ).astype(jnp.bfloat16),
        TP,
        scatter_dimension=0,
        tiled=True,
    )
    return (summed, log_weight)


def solution(mesh):
    torus = Mesh(mesh.devices.reshape(mesh.shape["sp"], 4, 2), ("sp", "tp_0", "tp_1"))
    return jax.shard_map(
        local,
        mesh=torus,
        in_specs=(
            P("sp", TP),
            P(),
            P("sp", TP),
            P("sp", TP),
            P("sp", TP),
            P("sp", TP),
            P("sp", TP),
            P(),
            P(),
            P(TP),
            P(None, TP),
            P(TP),
            P(TP),
            P("sp", TP),
            P("sp", TP),
        ),
        out_specs=(P(SP_TP, None), P(TP, "sp")),
        check_vma=False,
    )
```

profile of v0, /device:TPU:1, one launch (start us, length us, event | category | flops | bytes accessed | tf_op | source)
XLA Modules:
  0.0 250.0 jit_solution(3191542025246077211)
XLA Ops:
  7.2 1.5 concatenate.18
  8.8 2.5 %broadcast_in_dim.24 = bf16[4,1024,256]{2,1,0:T(8,128)(2,1)} broadcast(bf16[1024,256]{1,0:T(8,128)(2,1)} %param.15), dimensions={1,2} | broadcast | bytes 2621440 | tf_op jit(solution)/shard_map/broadcast_in_dim | solution.py:19
  11.3 4.8 %all-to-all-start = ((bf16[4,1024,256]{2,1,0:T(8,128)(2,1)}), bf16[4,1024,256]{2,1,0:T(8,128)(2,1)S(1)}, u32[]{:S(2)}, u32[]{:S(2)}) async-start(bf16[4,1024,256]{2,1,0:T(8,128)(2,1)} %broadcast_in_dim.24), calls=%async_computation | async-start | bytes 4194304 | tf_op jit(solution)/shard_map/all_to_all | solution.py:20
  16.9 1.0 broadcast_and_fusion
  17.9 18.7 %all-to-all-done = bf16[4,1024,256]{2,1,0:T(8,128)(2,1)S(1)} async-done(((bf16[4,1024,256]{2,1,0:T(8,128)(2,1)}), bf16[4,1024,256]{2,1,0:T(8,128)(2,1)S(1)}, u32[]{:S(2)}, u32[]{:S(2)}) %all-to-all-start) | async-done | bytes 2097184 | tf_op jit(solution)/shard_map/all_to_all | solution.py:20
  36.6 1.6 copy.71
  38.3 1.1 broadcast_in_dim.25
  39.4 13.5 %all_to_all.16 = bf16[2,4,1024,256]{3,1,2,0:T(4,128)(2,1)S(1)} all-to-all(bf16[2,4,1024,256]{3,1,2,0:T(4,128)(2,1)S(1)} %broadcast_in_dim.25), channel_id=1, replica_groups=mesh['sp'=64,'tp_0'=4,'tp_1'=2] {'tp_1'}, dimensions={0} | all-to-all | bytes 8388608 | tf_op jit(solution)/shard_map/all_to_all | solution.py:20
  52.9 0.8 copy_convert_fusion
  53.7 1.2 fusion.2
  54.9 2.0 copy-done
  56.9 3.3 %fusion.1 = bf16[8,1024,256]{2,1,0:T(8,128)(2,1)} fusion(f32[2,4,1024,256]{3,2,0,1:T(8,128)S(1)} %copy_convert_fusion, f32[8,256]{1,0:T(8,128)S(1)} %mul.455, f32[1024]{0:T(1024)S(1)} %add_rsqrt_fusion.2), kind=kLoop, calls=%fused_computation.3 | loop fusion | flops 6291456 | bytes 12595200 | tf_op jit(solution)/shard_map/convert.6
  60.2 6.5 %copy.76 = bf16[1024,8,256]{0,2,1:T(8,128)(2,1)} copy(bf16[1024,8,256]{2,0,1:T(8,128)(2,1)} %bitcast.172) | data formatting | bytes 8388608 | tf_op jit(solution)/shard_map/mul | solution.py:65
  66.7 9.1 %copy.73 = f32[1024,8,256]{0,2,1:T(8,128)} copy(f32[1024,8,256]{2,0,1:T(8,128)} %bitcast.171) | data formatting | bytes 16777216 | tf_op jit(solution)/shard_map/convert_element_type | solution.py:91
  75.8 5.2 %fusion.4 = bf16[1024,2048]{0,1:T(8,128)(2,1)} fusion(f32[1024,8,256]{0,2,1:T(8,128)} %copy.73, f32[2048]{0:T(1024)S(1)} %copy-done.4, f32[1024]{0:T(1024)S(1)} %add_rsqrt_fusion.2), kind=kLoop, calls=%fused_computation.7 | loop fusion | flops 6291456 | bytes 12595200 | tf_op jit(solution)/shard_map/convert_element_type | solution.py:91
  81.0 70.2 %all-gather.2.cloned.1.call-done = bf16[2048,768]{1,0:T(8,128)(2,1)} async-done(((bf16[32,768]{1,0:T(8,128)(2,1)}), bf16[2048,768]{1,0:T(8,128)(2,1)}) %all-gather.2.cloned.1.call-update) | async-done | bytes 3145744 | tf_op jit(solution)/shard_map/all_gather | solution.py:38
  151.2 2.0 slice_bitcast_fusion
  153.3 2.0 copy.77
  155.3 4.0 %multiply_reduce_fusion.1 = (f32[1024,2]{0,1:T(2,128)S(1)}, f32[1024,2,64]{0,2,1:T(8,128)}) fusion(bf16[1024,2048,1]{0,1,2:T(8,128)(2,1)} %bitcast.173, bf16[2,64,2048]{2,1,0:T(8,128)(2,1)} %bitcast.175), kind=kOutput, calls=%fused_computation.100 | convolution fusion | flops 537131008 | bytes 5251072 | tf_op jit(solution)/shard_map/dot_general | solution.py:96
  159.3 0.9 multiply_reduce_fusion.2
  160.2 1.3 fusion.11
  161.6 1.3 fusion.12
  163.1 2.0 collective-permute-start.1
  165.2 1.1 convolution_convert_fusion.1
  166.4 2.8 %collective-permute-start = (bf16[128,128]{0,1:T(8,128)(2,1)S(1)}, bf16[128,128]{0,1:T(8,128)(2,1)S(1)}, u32[]{:S(2)}, u32[]{:S(2)}) collective-permute-start(bf16[128,128]{0,1:T(8,128)(2,1)S(1)} %fusion.69), channel_id=1, source_target_pairs={{0,8},{8,16},{16,24},{24,32},{32,40},{40,48},{48,56},{56,64},{64,7... | collective-permute-start | bytes 98312 | tf_op jit(solution)/shard_map/ppermute | solution.py:48
  169.4 3.0 %fusion.79 = (f32[1024]{0:T(1024)S(1)}, f32[1024]{0:T(1024)S(1)}, f32[1024,128]{1,0:T(8,128)}) fusion(f32[1054,128]{1,0:T(8,128)S(1)} %maximum_convert_fusion, f32[128]{0:T(128)S(1)} %get-tuple-element.36, f32[128]{0:T(128)S(1)} %get-tuple-element.37, f32[128]{0:T(128)S(1)} %get-tuple-element.8, f32[128]{0:T(128)S(1)} %copy-done.7, f32[128]{0:T(128)S(1)} %copy-done.8, ...), kind=kLoop, calls=%fused_computation.185 | loop fusion | flops 8386560 | bytes 16801280 | tf_op jit(solution)/shard_map/reduce_sum | solution.py:154
  173.1 14.1 %all-to-all-start.2 = ((f32[8,1,2048]{2,1,0:T(1,128)}), f32[8,1,2048]{2,1,0:T(1,128)S(1)}, u32[]{:S(2)}, u32[]{:S(2)}) async-start(f32[8,1,2048]{2,1,0:T(1,128)} %broadcast_in_dim.29), calls=%async_computation.2 | async-start | bytes 131072 | tf_op jit(solution)/shard_map/all_to_all | solution.py:20
  187.5 1.7 fusion.5
  190.7 4.5 %fusion.48 = f32[1024,2048]{1,0:T(8,128)} fusion(bf16[2048,768]{1,0:T(8,128)(2,1)S(1)} %copy-done.2, bf16[16,8,8,128]{3,2,1,0:T(8,128)(2,1)S(1)} %bitcast.174), kind=kOutput, calls=%fused_computation.91 | convolution fusion | flops 536870912 | bytes 9175040 | tf_op jit(solution)/shard_map/dot_general | solution.py:162
  195.3 6.9 %add_convert_fusion = bf16[1024,2048]{1,0:T(8,128)(2,1)} fusion(f32[1024,2048]{1,0:T(8,128)} %fusion.48, bf16[2048,768]{1,0:T(8,128)(2,1)S(1)} %copy-done.2, f32[1024,128]{1,0:T(8,128)} %get-tuple-element.4, f32[128]{0:T(128)S(1)} %copy-done.25, f32[128]{0:T(128)S(1)} %copy-done.26, f32[1024]{0:T(1024)S(1)} %get-tuple-element.39, f32[1024]{0:T(1024)S(1)} %get-tuple-element.38), kind=kOutput, calls=%fused_computation.8 | convolution fusion | flops 542244864 | bytes 13640704 | tf_op jit(solution)/shard_map/dot_general | solution.py:166
  202.2 0.7 fusion.72
  202.9 40.2 %reduce-scatter.2.cloned.1.call-done = bf16[128,2048]{1,0:T(8,128)(2,1)} async-done(((bf16[1024,2048]{1,0:T(8,128)(2,1)}), bf16[128,2048]{1,0:T(8,128)(2,1)}) %reduce-scatter.2.cloned.1.call-update) | async-done | bytes 524304 | tf_op jit(solution)/shard_map/reduce_scatter | solution.py:163
  (86 shorter events, 3.6 us)
Async XLA Ops:
  7.2 8.9 %copy-start.4 = (f32[2048]{0:T(1024)S(1)}, f32[2048]{0:T(1024)}, u32[]{:S(2)}) copy-start(f32[2048]{0:T(1024)} %param.16) | copy-start | bytes 24580
  7.2 9.0 %copy-start.5 = (f32[31,128]{1,0:T(8,128)S(1)}, f32[31,128]{1,0:T(8,128)}, u32[]{:S(2)}) copy-start(f32[31,128]{1,0:T(8,128)} %param.25) | copy-start | bytes 47620
  7.2 144.1 %all-gather.2.cloned.1.call-start = ((), (), s32[]{:S(2)}) async-start(), calls=%async_computation.4 | async-start | bytes 3194880 | tf_op jit(solution)/shard_map/all_gather | solution.py:38
  11.3 25.4 %all-to-all-start = ((bf16[4,1024,256]{2,1,0:T(8,128)(2,1)}), bf16[4,1024,256]{2,1,0:T(8,128)(2,1)S(1)}, u32[]{:S(2)}, u32[]{:S(2)}) async-start(bf16[4,1024,256]{2,1,0:T(8,128)(2,1)} %broadcast_in_dim.24), calls=%async_computation | async-start | bytes 4194304 | tf_op jit(solution)/shard_map/all_to_all | solution.py:20
  53.7 3.2 %copy-start = (f32[2,4,1024,256]{3,2,0,1:T(8,128)}, f32[2,4,1024,256]{3,2,0,1:T(8,128)S(1)}, u32[]{:S(2)}) copy-start(f32[2,4,1024,256]{3,2,0,1:T(8,128)S(1)} %copy_convert_fusion) | copy-start | bytes 25165828
  151.2 8.1 %copy-start.2 = (bf16[2048,768]{1,0:T(8,128)(2,1)S(1)}, bf16[2048,768]{1,0:T(8,128)(2,1)}, u32[]{:S(2)}) copy-start(bf16[2048,768]{1,0:T(8,128)(2,1)} %all-gather.2.cloned.1.call-done) | copy-start | bytes 9437188
  155.3 4.0 %copy-start.1 = (bf16[1024,2048]{0,1:T(8,128)(2,1)S(1)}, bf16[1024,2048]{0,1:T(8,128)(2,1)}, u32[]{:S(2)}) copy-start(bf16[1024,2048]{0,1:T(8,128)(2,1)} %fusion.4) | copy-start | bytes 12582916
  161.6 3.6 %copy-start.24 = (f32[64]{0:T(128)S(1)}, f32[64]{0:T(128)}, u32[]{:S(2)}) copy-start(f32[64]{0:T(128)} %param.23) | copy-start | bytes 772
  162.9 6.3 %copy-start.7 = (f32[128]{0:T(128)S(1)}, f32[128]{0:T(128)}, u32[]{:S(2)}) copy-start(f32[128]{0:T(128)} %get-tuple-element.9) | copy-start | bytes 1540
  162.9 6.3 %copy-start.8 = (f32[128]{0:T(128)S(1)}, f32[128]{0:T(128)}, u32[]{:S(2)}) copy-start(f32[128]{0:T(128)} %get-tuple-element.10) | copy-start | bytes 1540
  162.9 6.3 %copy-start.9 = (f32[128]{0:T(128)S(1)}, f32[128]{0:T(128)}, u32[]{:S(2)}) copy-start(f32[128]{0:T(128)} %get-tuple-element.11) | copy-start | bytes 1540
  162.9 6.3 %copy-start.10 = (f32[128]{0:T(128)S(1)}, f32[128]{0:T(128)}, u32[]{:S(2)}) copy-start(f32[128]{0:T(128)} %get-tuple-element.12) | copy-start | bytes 1540
  162.9 6.3 %copy-start.11 = (f32[128]{0:T(128)S(1)}, f32[128]{0:T(128)}, u32[]{:S(2)}) copy-start(f32[128]{0:T(128)} %get-tuple-element.13) | copy-start | bytes 1540
  163.0 6.3 %copy-start.12 = (f32[128]{0:T(128)S(1)}, f32[128]{0:T(128)}, u32[]{:S(2)}) copy-start(f32[128]{0:T(128)} %get-tuple-element.14) | copy-start | bytes 1540
  163.0 6.3 %copy-start.13 = (f32[128]{0:T(128)S(1)}, f32[128]{0:T(128)}, u32[]{:S(2)}) copy-start(f32[128]{0:T(128)} %get-tuple-element.15) | copy-start | bytes 1540
  163.0 6.3 %copy-start.14 = (f32[128]{0:T(128)S(1)}, f32[128]{0:T(128)}, u32[]{:S(2)}) copy-start(f32[128]{0:T(128)} %get-tuple-element.16) | copy-start | bytes 1540
  163.0 6.3 %copy-start.15 = (f32[128]{0:T(128)S(1)}, f32[128]{0:T(128)}, u32[]{:S(2)}) copy-start(f32[128]{0:T(128)} %get-tuple-element.17) | copy-start | bytes 1540
  163.0 6.3 %copy-start.16 = (f32[128]{0:T(128)S(1)}, f32[128]{0:T(128)}, u32[]{:S(2)}) copy-start(f32[128]{0:T(128)} %get-tuple-element.18) | copy-start | bytes 1540
  163.0 6.3 %copy-start.17 = (f32[128]{0:T(128)S(1)}, f32[128]{0:T(128)}, u32[]{:S(2)}) copy-start(f32[128]{0:T(128)} %get-tuple-element.19) | copy-start | bytes 1540
  163.0 6.3 %copy-start.18 = (f32[128]{0:T(128)S(1)}, f32[128]{0:T(128)}, u32[]{:S(2)}) copy-start(f32[128]{0:T(128)} %get-tuple-element.20) | copy-start | bytes 1540
  163.0 6.3 %copy-start.19 = (f32[128]{0:T(128)S(1)}, f32[128]{0:T(128)}, u32[]{:S(2)}) copy-start(f32[128]{0:T(128)} %get-tuple-element.21) | copy-start | bytes 1540
  163.0 6.3 %copy-start.20 = (f32[128]{0:T(128)S(1)}, f32[128]{0:T(128)}, u32[]{:S(2)}) copy-start(f32[128]{0:T(128)} %get-tuple-element.22) | copy-start | bytes 1540
  163.1 6.3 %copy-start.21 = (f32[128]{0:T(128)S(1)}, f32[128]{0:T(128)}, u32[]{:S(2)}) copy-start(f32[128]{0:T(128)} %get-tuple-element.23) | copy-start | bytes 1540
  163.1 6.3 %copy-start.22 = (f32[128]{0:T(128)S(1)}, f32[128]{0:T(128)}, u32[]{:S(2)}) copy-start(f32[128]{0:T(128)} %get-tuple-element.24) | copy-start | bytes 1540
  163.1 6.3 %copy-start.23 = (f32[128]{0:T(128)S(1)}, f32[128]{0:T(128)}, u32[]{:S(2)}) copy-start(f32[128]{0:T(128)} %get-tuple-element.25) | copy-start | bytes 1540
  163.1 6.1 %collective-permute-start.1 = (bf16[30,128]{1,0:T(8,128)(2,1)S(1)}, bf16[30,128]{1,0:T(8,128)(2,1)S(1)}, u32[]{:S(2)}, u32[]{:S(2)}) collective-permute-start(bf16[30,128]{1,0:T(8,128)(2,1)S(1)} %slice.323), channel_id=1, source_target_pairs={{0,8},{8,16},{16,24},{24,32},{32,40},{40,48},{48,56},{56,64},{64,7... | collective-permute-start | bytes 23048 | tf_op jit(solution)/shard_map/ppermute | solution.py:48
  166.4 20.8 %collective-permute-start = (bf16[128,128]{0,1:T(8,128)(2,1)S(1)}, bf16[128,128]{0,1:T(8,128)(2,1)S(1)}, u32[]{:S(2)}, u32[]{:S(2)}) collective-permute-start(bf16[128,128]{0,1:T(8,128)(2,1)S(1)} %fusion.69), channel_id=1, source_target_pairs={{0,8},{8,16},{16,24},{24,32},{32,40},{40,48},{48,56},{56,64},{64,7... | collective-permute-start | bytes 98312 | tf_op jit(solution)/shard_map/ppermute | solution.py:48
  172.4 16.8 %copy-start.6 = (f32[2]{0:T(128)S(1)}, f32[2]{0:T(128)}, u32[]{:S(2)}) copy-start(f32[2]{0:T(128)} %param.24) | copy-start | bytes 28
  173.1 22.2 %all-to-all-start.2 = ((f32[8,1,2048]{2,1,0:T(1,128)}), f32[8,1,2048]{2,1,0:T(1,128)S(1)}, u32[]{:S(2)}, u32[]{:S(2)}) async-start(f32[8,1,2048]{2,1,0:T(1,128)} %broadcast_in_dim.29), calls=%async_computation.2 | async-start | bytes 131072 | tf_op jit(solution)/shard_map/all_to_all | solution.py:20
  187.2 56.0 %reduce-scatter.2.cloned.1.call-start = ((), (), s32[]{:S(2)}) async-start(), calls=%async_computation.5 | async-start | bytes 4718592 | tf_op jit(solution)/shard_map/reduce_scatter | solution.py:163
  190.7 4.6 %copy-start.25 = (f32[128]{0:T(128)S(1)}, f32[128]{0:T(128)}, u32[]{:S(2)}) copy-start(f32[128]{0:T(128)} %param.27) | copy-start | bytes 1540
  190.7 4.6 %copy-start.26 = (f32[128]{0:T(128)S(1)}, f32[128]{0:T(128)}, u32[]{:S(2)}) copy-start(f32[128]{0:T(128)} %param.26) | copy-start | bytes 1540
  (1 other events, 2.0 us)
Sparse Core Ops, SparseCore 0:
  11.5 139.6 all-gather.1
  202.4 40.7 reduce-scatter.1
where the time goes:
time: 252 us; the launch traced here: 250 us
  waiting for transfers between devices  129 us (51%)
  local copies, waits for them, and re-layouts  30.2 us (12%)
  starting transfers between devices  23.8 us (9%)
  matrix products  22.4 us (9%)
  other arithmetic  16.3 us (6%)
  between operations  14.6 us (6%)
  blocking collectives  13.5 us (5%)
    all_gather x1, waiting for transfers between devices, side_by_side(): whole, at, outs = (lax.all_gather(both, axis, axis=dim, tiled=True), 0, [])  70.2 us
    reduce_scatter x1, waiting for transfers between devices, local(): lax.psum_scatter((result + lax.dot_general(conv_rows, conv_back, contract...  40.2 us
    all_to_all x2, starting transfers between devices, sent_to_all(): return lax.all_to_all(copies, axis, split_axis=0, concat_axis=0, tiled=True)  19 us
    all_to_all x2, waiting for transfers between devices, sent_to_all(): return lax.all_to_all(copies, axis, split_axis=0, concat_axis=0, tiled=True)  18.7 us
    all_to_all x1, blocking collectives, sent_to_all(): return lax.all_to_all(copies, axis, split_axis=0, concat_axis=0, tiled=True)  13.5 us
    convert_element_type x1, local copies, waits for them, and re-layouts, local(): gathered.astype(jnp.float32)  9.12 us
    dot_general x5, matrix products, local(): jnp.dot(normed, weight, preferred_element_type=jnp.float32)  8.61 us
    dot_general x1, matrix products, local(): lax.dot_general(conv_rows, conv_back, contract, preferred_element_type=jn...  6.88 us
  transfers between devices with their start and end apart: 6, of which 3 were waited for; matrix products, arithmetic and copies ran while one was open for 19% of the time, Pallas kernels for 0%

commit v1 on v0

v1 whole, which is shorter than its diff:
```python
import functools

import jax
import jax.numpy as jnp
from jax import lax
from jax.experimental import pallas as pl
from jax.experimental.pallas import tpu as pltpu
from jax.sharding import PartitionSpec as P

MESH = pl.DeviceIdType.MESH
HEAD = 64
CH = 1024
KW = 31
WINDOW = 128
EPS = 1e-06
NX, NC, NY = 4, 2, 4
LANES = 128
RIM = 32
PIECES = 4
BF = jnp.bfloat16
F32 = jnp.float32


def kernel(
    nz,
    tok_in,
    norm_gain,
    w_query,
    w_key,
    w_value,
    w_glu_a,
    w_glu_b,
    q_gain,
    k_gain,
    sink,
    conv_taps,
    chan_gain,
    chan_bias,
    w_attn_back,
    w_conv_back,
    out,
    log_weight,
    tok,
    nrm,
    wa,
    wb,
    qp,
    kvx,
    ext,
    conv,
    act,
    stats,
    lines,
    own,
    snd,
    pre,
    relay_a,
    relay_b,
    fin,
    tok_sem,
    own_d2d,
    x_sem,
    xr_sem,
    d2d_sem,
    ya_sem,
    up_a,
    dn_a,
    up_b,
    dn_b,
    by_r,
    by_l,
    br_r,
    br_l,
    halo_sem,
    stat_sem,
    pre_sem,
    rs_sem,
):
    sp = lax.axis_index("sp")
    tp = lax.axis_index("tp")
    n_sp = nz * NY
    z, y = sp // NY, sp % NY
    x, c = tp // NC, tp % NC
    rows = tok_in.shape[0]
    half = nz // 2
    piece = rows // PIECES
    pending = []

    def at(zz, yy, xx, cc):
        return (lax.rem(zz + nz, nz) * NY + lax.rem(yy + NY, NY), lax.rem(xx + NX, NX) * NC + cc)

    def send(src, dst, sems, index, where):
        copy = pltpu.make_async_remote_copy(
            src_ref=src,
            dst_ref=dst,
            send_sem=sems.at[(0, *index)],
            recv_sem=sems.at[(1, *index)],
            device_id=where,
            device_id_type=MESH,
        )
        copy.start()
        pending.append(copy)

    def landed(ref, sems, index):
        pltpu.make_async_remote_copy(
            src_ref=ref,
            dst_ref=ref,
            send_sem=sems.at[(0, *index)],
            recv_sem=sems.at[(1, *index)],
            device_id=partner,
            device_id_type=MESH,
        ).wait_recv()

    z_up, z_dn = at(z + 1, y, x, c), at(z - 1, y, x, c)
    y_up, y_dn = at(z, y + 1, x, c), at(z, y - 1, x, c)
    x_up, x_dn = at(z, y, x + 1, c), at(z, y, x - 1, c)
    partner = (sp, x * NC + (1 - c))
    following = (lax.rem(sp + 1, n_sp), tp)
    preceding = (lax.rem(sp + n_sp - 1, n_sp), tp)

    load = pltpu.make_async_copy(tok_in, tok.at[tp], tok_sem)
    load.start()

    def weight_rows(zz, yy):
        block = lax.rem(zz + 2 * nz, nz) * NY + lax.rem(yy + NY, NY)
        return pl.ds(pl.multiple_of(block * 32, 32), 32)

    mine = weight_rows(z, y)
    wa[mine, :LANES] = w_query[...]
    wa[mine, LANES:] = jnp.concatenate([w_key[...], w_value[...]], axis=1)
    wb[mine, :LANES] = w_glu_a[...]
    wb[mine, LANES : 2 * LANES] = w_glu_b[...]
    wb[mine, 2 * LANES : 3 * LANES] = w_attn_back[...]
    wb[mine, 3 * LANES :] = w_conv_back[...]

    barrier = pltpu.get_barrier_semaphore()
    peers = [(sp, lax.rem(tp + k, NX * NC)) for k in range(1, NX * NC)]
    peers += [at(z, y + k, x, c) for k in range(1, NY)]
    peers += [z_up, z_dn, following, preceding]
    for peer in peers:
        pl.semaphore_signal(barrier, inc=1, device_id=peer, device_id_type=MESH)
    pl.semaphore_wait(barrier, len(peers))

    def wa_at(zz, yy):
        return wa.at[weight_rows(zz, yy)]

    def wb_at(zz, yy):
        return wb.at[weight_rows(zz, yy)]

    offsets = (0, 1, 3, 2)

    def a_up(step, j):
        if step < half - 1 or (step == half - 1 and j < 2):
            block = wa_at(z - step, y - offsets[j])
            send(block, block, up_a, (step, j), z_up)

    def a_dn(step, j):
        if step < half - 1 or (step == half - 1 and j >= 2):
            block = wa_at(z + step, y - offsets[j])
            send(block, block, dn_a, (step, j), z_dn)

    def b_up(step):
        if step < half:
            block = wb_at(z - step, y)
            send(block, block, up_b, (step,), z_up)

    def b_dn(step):
        if step < half - 1:
            block = wb_at(z + step, y)
            send(block, block, dn_b, (step,), z_dn)

    def shift(n):
        return -n - 1 if n < half else n - half

    def b_y(n):
        block = wb_at(z + shift(n), y)
        send(block, block, by_r, (n,), y_up)
        send(block, block, by_l, (n,), y_dn)

    def b_relay(n):
        if n < half:
            block = wb_at(z + shift(n), y - 1)
            landed(block, by_r, (n,))
            send(block, block, br_r, (n,), y_up)
        else:
            block = wb_at(z + shift(n), y + 1)
            landed(block, by_l, (n,))
            send(block, block, br_l, (n - half,), y_dn)

    a_up(0, 0)
    a_dn(0, 0)
    for k in (1, 3, 2):
        send(wa_at(z, y), wa_at(z, y), ya_sem, (k,), at(z, y + k, x, c))
    b_up(0)
    b_dn(0)
    b_y(half)

    def tok_at(xx, cc, i):
        return tok.at[lax.rem(xx + NX, NX) * NC + cc, pl.ds(i * piece, piece)]

    load.wait()
    order_up, order_dn = (0, 1, 2, 3), (2, 3, 0, 1)
    for i, j in zip(order_up, order_dn):
        send(tok_at(x, c, i), tok_at(x, c, i), x_sem, (0, i), x_up)
        send(tok_at(x, c, j), tok_at(x, c, j), x_sem, (1, j), x_dn)
    send(tok.at[tp], tok.at[tp], own_d2d, (), partner)

    def to_partner(k, xx, i):
        send(tok_at(xx, c, i), tok_at(xx, c, i), d2d_sem, (k, i), partner)

    def tokens_step(n):
        if n < PIECES:
            i, j = order_up[n], order_dn[n]
            landed(tok_at(x - 1, c, i), x_sem, (0, i))
            if n < PIECES // 2:
                send(tok_at(x - 1, c, i), tok_at(x - 1, c, i), xr_sem, (i,), x_up)
            to_partner(0, x - 1, i)
            landed(tok_at(x + 1, c, j), x_sem, (1, j))
            if n < PIECES // 2:
                send(tok_at(x + 1, c, j), tok_at(x + 1, c, j), xr_sem, (j,), x_dn)
            to_partner(1, x + 1, j)
        elif n < PIECES + PIECES // 2:
            for i in (order_up[n - PIECES], order_dn[n - PIECES]):
                landed(tok_at(x + 2, c, i), xr_sem, (i,))
                to_partner(2, x + 2, i)

    for j in range(1, NY):
        k = offsets[j]
        landed(wa_at(z, y - k), ya_sem, (k,))
        a_up(0, j)
        a_dn(0, j)
    for step in range(half):
        landed(wb_at(z - step - 1, y), up_b, (step,))
        b_up(step + 1)
        b_y(step)
        if step < half - 1:
            landed(wb_at(z + step + 1, y), dn_b, (step,))
            b_dn(step + 1)
            b_y(half + step + 1)
        for j in range(NY):
            if step < half - 1 or j < 2:
                landed(wa_at(z - step - 1, y - offsets[j]), up_a, (step, j))
                a_up(step + 1, j)
            if step < half - 1 or j >= 2:
                landed(wa_at(z + step + 1, y - offsets[j]), dn_a, (step, j))
                a_dn(step + 1, j)
        b_relay(half + step)
        if step > 0:
            b_relay(step - 1)
        if step > 0:
            tokens_step(step - 1)
    b_relay(half - 1)
    for n in range(half - 1, PIECES + PIECES // 2):
        tokens_step(n)

    landed(tok.at[x * NC + 1 - c], own_d2d, ())
    for k, xx in ((0, x - 1), (1, x + 1), (2, x + 2)):
        for i in range(PIECES):
            landed(tok_at(xx, 1 - c, i), d2d_sem, (k, i))

    tile = 128
    gains = [norm_gain[i : i + 1, :] for i in range(NX * NC)]

    def norm_tile(t, carry):
        at_rows = pl.ds(pl.multiple_of(t * tile, tile), tile)
        total = jnp.zeros((tile, 256), F32)
        for i in range(NX * NC):
            v = tok[i, at_rows, :].astype(F32)
            total = total + v * v
        scale = lax.rsqrt(jnp.sum(total, axis=1, keepdims=True) * (1.0 / 2048) + EPS)
        for i in range(NX * NC):
            v = tok[i, at_rows, :].astype(F32)
            nrm[at_rows, i * 256 : (i + 1) * 256] = (v * scale * gains[i]).astype(BF)
        return carry

    lax.fori_loop(0, rows // tile, norm_tile, 0)

    for n in range(half, 2 * half):
        landed(wb_at(z + shift(n), y - 1), by_r, (n,))
    for n in range(half):
        landed(wb_at(z + shift(n), y + 1), by_l, (n,))
    for n in range(half):
        landed(wb_at(z + shift(n), y + 2), br_r, (n,))
        landed(wb_at(z + shift(half + n), y + 2), br_l, (n,))

    big = 256
    low = lax.broadcasted_iota(jnp.int32, (big, LANES), 1) < HEAD

    def project(t):
        at_rows = pl.ds(pl.multiple_of(t * big, big), big)
        normed = nrm[at_rows, :]
        first = jnp.dot(normed, wa[...], preferred_element_type=F32)
        second = jnp.dot(normed, wb[:, :256], preferred_element_type=F32)
        q, kv = first[:, :LANES], first[:, LANES:]
        squares = q * q
        mean0 = jnp.sum(jnp.where(low, squares, 0.0), axis=1, keepdims=True) * (1.0 / HEAD)
        mean1 = jnp.sum(jnp.where(low, 0.0, squares), axis=1, keepdims=True) * (1.0 / HEAD)
        qn = q * jnp.where(low, lax.rsqrt(mean0 + EPS), lax.rsqrt(mean1 + EPS)) * q_gain[...]
        qp[0, at_rows, :] = jnp.where(low, qn, 0.0).astype(BF)
        qp[1, at_rows, :] = jnp.where(low, pltpu.roll(qn, HEAD, 1), 0.0).astype(BF)
        mean = jnp.sum(jnp.where(low, kv * kv, 0.0), axis=1, keepdims=True) * (1.0 / HEAD)
        kn = kv * lax.rsqrt(mean + EPS) * k_gain[...]
        kvx[pl.ds(pl.multiple_of(t * big + WINDOW, WINDOW), big), :] = jnp.where(low, kn, kv).astype(BF)
        a, b = second[:, :LANES], second[:, LANES:]
        gated = (a * (1.0 / (1.0 + jnp.exp(-b)))).astype(BF).astype(F32)
        ext[pl.ds(pl.multiple_of(t * big + RIM, RIM), big), :] = gated

    tiles = rows // big
    project(tiles - 1)
    send(kvx.at[pl.ds(rows, WINDOW)], kvx.at[pl.ds(0, WINDOW)], halo_sem, (0,), following)
    send(ext.at[pl.ds(rows, RIM)], ext.at[pl.ds(0, RIM)], halo_sem, (1,), following)

    def project_step(t, carry):
        project(t)
        return carry

    lax.fori_loop(0, tiles - 1, project_step, 0)
    landed(ext.at[pl.ds(0, RIM)], halo_sem, (1,))
    ext[:RIM, :] = jnp.where(sp > 0, ext[:RIM, :], 0.0)

    eye = lax.broadcasted_iota(jnp.int32, (LANES, LANES), 0) == lax.broadcasted_iota(
        jnp.int32, (LANES, LANES), 1
    )
    blocks = rows // LANES
    for t in range(blocks):
        total = jnp.zeros((LANES, LANES), F32)
        for j in range(KW):
            start = t * LANES + RIM - (KW - 1) + j
            total = total + conv_taps[j : j + 1, :] * ext[start : start + LANES, :]
        conv[t * LANES : (t + 1) * LANES, :] = total
        for k, terms in enumerate((total, total * total)):
            column = jnp.sum(terms, axis=1, keepdims=True)
            line = jnp.sum(jnp.where(eye, column, 0.0), axis=0, keepdims=True)
            stats[tp, k * blocks + t : k * blocks + t + 1, :] = line
    for k in range(1, NX * NC):
        send(stats.at[tp], stats.at[tp], stat_sem, (k,), (sp, lax.rem(tp + k, NX * NC)))
    landed(kvx.at[pl.ds(0, WINDOW)], halo_sem, (0,))

    hq = 2 * WINDOW
    key_index = lax.broadcasted_iota(jnp.int32, (hq, hq), 0)
    query_index = lax.rem(lax.broadcasted_iota(jnp.int32, (hq, hq), 1), WINDOW)
    band = (key_index > query_index) & (key_index <= query_index + WINDOW)
    lane_row = lax.broadcasted_iota(jnp.int32, (1, hq), 1)
    sinks = jnp.where(lane_row < WINDOW, sink[0], sink[1])
    low_w = lax.broadcasted_iota(jnp.int32, (WINDOW, LANES), 1) < HEAD

    def attend(b):
        r0 = pl.multiple_of(b * WINDOW, WINDOW)
        keys = kvx[pl.ds(r0, hq), :]
        queries = jnp.concatenate([qp[0, pl.ds(r0, WINDOW), :], qp[1, pl.ds(r0, WINDOW), :]], axis=0)
        scores = lax.dot_general(keys, queries, (((1,), (1,)), ((), ())), preferred_element_type=F32)
        scores = scores * HEAD ** (-0.5)
        least = jnp.where(sp * rows + b * WINDOW > 0, 0, WINDOW)
        visible = band & (key_index >= least)
        largest = jnp.max(jnp.where(visible, scores, -jnp.inf), axis=0, keepdims=True)
        largest = jnp.maximum(largest, sinks)
        weights = jnp.where(visible, jnp.exp(scores - largest), 0.0)
        weight_sum = jnp.sum(weights, axis=0, keepdims=True) + jnp.exp(sinks - largest)
        line = largest + jnp.log(weight_sum)
        log_weight[0:1, pl.ds(r0, WINDOW)] = line[:, :WINDOW]
        log_weight[1:2, pl.ds(r0, WINDOW)] = line[:, WINDOW:]
        shares = (weights * (1.0 / weight_sum)).astype(BF)
        mixed = lax.dot_general(shares, keys, (((0,), (0,)), ((), ())), preferred_element_type=F32)
        mixed = jnp.where(low_w, pltpu.roll(mixed[:WINDOW], HEAD, 1), mixed[WINDOW:])
        act[pl.ds(r0, WINDOW), :LANES] = mixed.astype(BF)

    def channel_norm(t, center, scale):
        at_rows = pl.ds(pl.multiple_of(t * LANES, LANES), LANES)
        columns = []
        for lines in (center, scale):
            columns.append(jnp.sum(jnp.where(eye, lines, 0.0), axis=1, keepdims=True))
        normal = (conv[at_rows, :] - columns[0]) * columns[1] * chan_gain[...] + chan_bias[...]
        act[at_rows, LANES:] = (normal * (1.0 / (1.0 + jnp.exp(-normal)))).astype(BF)

    def attend_group(o):
        g = lax.rem(x + o, NX)

        def one(i, carry):
            attend(g * NC + i)
            return carry

        lax.fori_loop(0, NC, one, 0)

    def project_back(o):
        g = lax.rem(x + o, NX)
        for i in range(NC):
            t = g * NC + i
            channel_norm(t, lines[pl.ds(t, 1), :], lines[pl.ds(t + blocks, 1), :])
        keep = act[pl.ds(pl.multiple_of((g * NC + c) * LANES, LANES), LANES), :]
        give = act[pl.ds(pl.multiple_of((g * NC + 1 - c) * LANES, LANES), LANES), :]
        both = jnp.concatenate([keep, give], axis=0)
        for n in range(4):
            cols = slice(n * 512, (n + 1) * 512)
            part = lax.dot_general(
                both, wb[cols, 256:], (((1,), (1,)), ((), ())), preferred_element_type=F32
            ).astype(BF)
            own[o, :, cols] = part[:LANES]
            snd[o, :, cols] = part[LANES:]
        send(snd.at[o], pre.at[o], pre_sem, (o,), partner)

    attend_group(2)
    for k in range(1, NX * NC):
        other = lax.rem(tp + NX * NC - k, NX * NC)
        landed(stats.at[other], stat_sem, (k,))
    sums = jnp.sum(stats[...], axis=0)
    center = sums[:blocks] * (1.0 / CH)
    spread = sums[blocks:] * (1.0 / CH) - center * center
    lines[:blocks, :] = center
    lines[blocks:, :] = lax.rsqrt(spread + EPS)

    project_back(2)
    hr = LANES // 2

    def pair(o, lo):
        return own[o, lo : lo + hr, :].astype(F32) + pre[o, lo : lo + hr, :].astype(F32)

    attend_group(1)
    project_back(1)
    landed(pre.at[2], pre_sem, (2,))
    own[2, :hr, :] = pair(2, 0).astype(BF)
    send(own.at[2, pl.ds(0, hr)], relay_a, rs_sem, (0,), x_up)
    own[2, hr:, :] = pair(2, hr).astype(BF)
    send(own.at[2, pl.ds(hr, hr)], relay_b, rs_sem, (1,), x_dn)
    attend_group(3)
    project_back(3)
    landed(pre.at[1], pre_sem, (1,))
    own[1, hr:, :] = pair(1, hr).astype(BF)
    send(own.at[1, pl.ds(hr, hr)], fin.at[0, pl.ds(hr, hr)], rs_sem, (2,), x_up)
    landed(pre.at[3], pre_sem, (3,))
    own[3, :hr, :] = pair(3, 0).astype(BF)
    send(own.at[3, pl.ds(0, hr)], fin.at[1, pl.ds(0, hr)], rs_sem, (3,), x_dn)
    attend_group(0)
    project_back(0)
    landed(relay_a, rs_sem, (0,))
    own[1, :hr, :] = (pair(1, 0) + relay_a[...].astype(F32)).astype(BF)
    send(own.at[1, pl.ds(0, hr)], fin.at[0, pl.ds(0, hr)], rs_sem, (4,), x_up)
    landed(relay_b, rs_sem, (1,))
    own[3, hr:, :] = (pair(3, hr) + relay_b[...].astype(F32)).astype(BF)
    send(own.at[3, pl.ds(hr, hr)], fin.at[1, pl.ds(hr, hr)], rs_sem, (5,), x_dn)
    landed(pre.at[0], pre_sem, (0,))
    for lo, first, second in ((hr, (0, 2), (1, 5)), (0, (1, 3), (0, 4))):
        for k, i in (first, second):
            landed(fin.at[k, pl.ds(lo, hr)], rs_sem, (i,))
        total = pair(0, lo)
        for k in range(2):
            total = total + fin[k, lo : lo + hr, :].astype(F32)
        out[lo : lo + hr, :] = total.astype(BF)

    for copy in pending:
        copy.wait_send()


def local(
    tokens,
    norm_gain,
    w_query,
    w_key,
    w_value,
    w_glu_a,
    w_glu_b,
    q_gain,
    k_gain,
    sink_logit,
    conv_taps,
    chan_gain,
    chan_bias,
    w_attn_back,
    w_conv_back,
):
    rows, width = tokens.shape
    model = norm_gain.shape[0]
    nz = lax.axis_size("sp") // NY
    half = nz // 2
    n_tp = NX * NC
    blocks = rows // LANES
    vmem = pl.BlockSpec(memory_space=pltpu.VMEM)
    dma = pltpu.SemaphoreType.DMA
    return pl.pallas_call(
        functools.partial(kernel, nz),
        out_shape=(
            jax.ShapeDtypeStruct((LANES, model), BF),
            jax.ShapeDtypeStruct((2, rows), F32),
        ),
        in_specs=[pl.BlockSpec(memory_space=pltpu.HBM)]
        + [vmem] * 8
        + [pl.BlockSpec(memory_space=pltpu.SMEM)]
        + [vmem] * 5,
        out_specs=(vmem, vmem),
        scratch_shapes=[
            pltpu.VMEM((n_tp, rows, width), BF),
            pltpu.VMEM((rows, model), BF),
            pltpu.VMEM((model, 256), BF),
            pltpu.VMEM((model, 512), BF),
            pltpu.VMEM((2, rows, LANES), BF),
            pltpu.VMEM((rows + WINDOW, LANES), BF),
            pltpu.VMEM((rows + RIM, LANES), F32),
            pltpu.VMEM((rows, LANES), F32),
            pltpu.VMEM((rows, 256), BF),
            pltpu.VMEM((n_tp, 2 * blocks, LANES), F32),
            pltpu.VMEM((2 * blocks, LANES), F32),
            pltpu.VMEM((NX, LANES, model), BF),
            pltpu.VMEM((NX, LANES, model), BF),
            pltpu.VMEM((NX, LANES, model), BF),
            pltpu.VMEM((LANES // 2, model), BF),
            pltpu.VMEM((LANES // 2, model), BF),
            pltpu.VMEM((2, LANES, model), BF),
            dma,
            dma((2,)),
            dma((2, 2, PIECES)),
            dma((2, PIECES)),
            dma((2, 3, PIECES)),
            dma((2, NY)),
            dma((2, half, NY)),
            dma((2, half, NY)),
            dma((2, half)),
            dma((2, half)),
            dma((2, 2 * half)),
            dma((2, 2 * half)),
            dma((2, half)),
            dma((2, half)),
            dma((2, 2)),
            dma((2, n_tp)),
            dma((2, NX)),
            dma((2, 6)),
        ],
        compiler_params=pltpu.CompilerParams(
            collective_id=0, has_side_effects=True, vmem_limit_bytes=60 * 1024 * 1024
        ),
    )(
        tokens,
        norm_gain.reshape(n_tp, width),
        w_query,
        w_key,
        w_value,
        w_glu_a,
        w_glu_b,
        jnp.concatenate([q_gain, q_gain]).reshape(1, LANES),
        jnp.concatenate([k_gain, k_gain]).reshape(1, LANES),
        sink_logit,
        conv_taps,
        chan_gain.reshape(1, LANES),
        chan_bias.reshape(1, LANES),
        w_attn_back,
        w_conv_back,
    )


def solution(mesh):
    return jax.shard_map(
        local,
        mesh=mesh,
        in_specs=(
            P("sp", "tp"),
            P(),
            P("sp", "tp"),
            P("sp", "tp"),
            P("sp", "tp"),
            P("sp", "tp"),
            P("sp", "tp"),
            P(),
            P(),
            P("tp"),
            P(None, "tp"),
            P("tp"),
            P("tp"),
            P("sp", "tp"),
            P("sp", "tp"),
        ),
        out_specs=(P(("sp", "tp"), None), P("tp", "sp")),
        check_vma=False,
    )
```

time: 252 us -> 89.9 us (0.36)
  waiting for transfers between devices: 129 us -> 0 us
  Pallas kernels: 0 us -> 84.5 us
  local copies, waits for them, and re-layouts: 30.2 us -> 3.09 us
  starting transfers between devices: 23.8 us -> 0 us
  matrix products: 22.4 us -> 0 us
  other arithmetic: 16.3 us -> 1.39 us
  between operations: 14.6 us -> 0.66 us
  blocking collectives: 13.5 us -> 0 us
    pallas_call x0 -> x1, Pallas kernels: none -> 84.5 us  [local(): pl.pallas_call(functools.partial(kernel, nz), out_shape=(jax.ShapeDtypeSt...]
    all_gather x1 -> x0, waiting for transfers between devices: 70.2 us -> none  [side_by_side(): whole, at, outs = (lax.all_gather(both, axis, axis=dim, tiled=True), 0, [])]
    reduce_scatter x1 -> x0, waiting for transfers between devices: 40.2 us -> none  [local(): lax.psum_scatter((result + lax.dot_general(conv_rows, conv_back, contract...]
    dot_general x9 -> x0, matrix products: 22.4 us -> none  [the longest x5 8.61 us: local(): jnp.dot(normed, weight, preferred_element_type=jnp.float32)]
    all_to_all x2 -> x0, starting transfers between devices: 19 us -> none  [sent_to_all(): return lax.all_to_all(copies, axis, split_axis=0, concat_axis=0, tiled=True)]
    all_to_all x2 -> x0, waiting for transfers between devices: 18.7 us -> none  [sent_to_all(): return lax.all_to_all(copies, axis, split_axis=0, concat_axis=0, tiled=True)]
    all_to_all x1 -> x0, blocking collectives: 13.5 us -> none  [sent_to_all(): return lax.all_to_all(copies, axis, split_axis=0, concat_axis=0, tiled=True)]
    convert_element_type x2 -> x0, local copies, waits for them, and re-layouts: 9.3 us -> none  [the longest x1 9.12 us: local(): gathered.astype(jnp.float32)]
  transfers between devices with their start and end apart: 6 -> 0, of which waited for: 3 -> 0; matrix products, arithmetic and copies ran while one was open for 19% -> 0% of each run, Pallas kernels for 0% -> 0%
where the time goes in v1:
time: 89.9 us; the launch traced here: 89.6 us
  Pallas kernels  84.5 us (94%)
  local copies, waits for them, and re-layouts  3.09 us (3%)
  other arithmetic  1.39 us (2%)
    pallas_call x1, Pallas kernels, local(): pl.pallas_call(functools.partial(kernel, nz), out_shape=(jax.ShapeDtypeSt...  84.5 us
    unnamed x6, local copies, waits for them, and re-layouts  2.49 us

profile of v1, /device:TPU:1, one launch (start us, length us, event | category | flops | bytes accessed | tf_op | source)
XLA Modules:
  0.0 89.6 jit_solution(510538129462279651)
XLA Ops:
  0.6 0.0 copy-start
  0.6 1.4 %maximum_bitcast_fusion = (f32[1,128]{1,0:T(1,128)}, f32[1,128]{1,0:T(1,128)}) fusion(f32[64]{0:T(128)} %param.22, f32[64]{0:T(128)} %param.23), kind=kLoop, calls=%fused_computation | loop fusion | flops 256 | bytes 1536 | tf_op jit(solution)/shard_map/reshape | solution.py:537
  2.0 0.0 copy-done
  2.0 0.6 reshape.19.norm_gain
  2.6 84.5 %shard_map.158 = (bf16[128,2048]{1,0:T(8,128)(2,1)}, f32[2,1024]{1,0:T(2,128)}) custom-call(bf16[1024,256]{1,0:T(8,128)(2,1)} %tok_in.1, f32[8,256]{1,0:T(8,128)} %reshape.19.norm_gain, bf16[32,128]{1,0:T(8,128)(2,1)} %w_query.1, bf16[32,64]{1,0:T(8,128)(2,1)} %w_key.1, bf16[32,64]{1,0:T(8,128)(2,1)} %w_value.1, bf16[32,128]{1,0:T(8,128)(2,1)} %w_glu_a.1, ...), custom_call_target="tpu_custom_call" | custom-call | tf_op jit(solution)/shard_map/pallas_call | solution.py:478
  87.1 0.0 copy-start.1
  87.1 1.9 %copy.19 = bf16[128,2048]{1,0:T(8,128)(2,1)} copy(bf16[128,2048]{1,0:T(8,128)(2,1)} %get-tuple-element.6) | data formatting | bytes 1048576
  89.0 0.0 copy-done.1
  89.0 0.6 copy.20
Async XLA Ops:
  0.6 1.4 %copy-start = (f32[2048]{0:T(1024)S(1)}, f32[2048]{0:T(1024)}, u32[]{:S(2)}) copy-start(f32[2048]{0:T(1024)} %param.16) | copy-start | bytes 24580
  87.1 1.9 %copy-start.1 = (f32[2,1024]{1,0:T(2,128)S(1)}, f32[2,1024]{1,0:T(2,128)}, u32[]{:S(2)}) copy-start(f32[2,1024]{1,0:T(2,128)} %get-tuple-element.7) | copy-start | bytes 24580
